TPU v7x, 512 devices: a whole 4x8x8 slice. The times are simulated.
512 devices in a mesh: sp: 128 (over z, y, core), tp: 4 (over x).
Axes of the slice: x: 4, y: 8, z: 8, core: 2. Of those that a mesh axis runs over, the one named last changes fastest.
Arguments:
- tokens: bfloat16 [24576, 2048], P('sp'), may hold values from -10 to 10
- w_query: bfloat16 [2048, 1024], P(None, 'tp'), may hold values from -0.125 to 0.125
- w_key: bfloat16 [2048, 256], P(None, 'tp'), may hold values from -0.125 to 0.125
- w_value: bfloat16 [2048, 256], P(None, 'tp'), may hold values from -0.125 to 0.125
- w_output: bfloat16 [1024, 2048], P('tp'), may hold values from -0.1875 to 0.1875
- query_gain: float32 [64], replicated, may hold values from 0.4 to 9
- key_gain: float32 [64], replicated, may hold values from 0.4 to 9
Outputs:
- mixed_out: bfloat16 [24576, 2048], P(('sp', 'tp'))
- log_sums: float32 [16, 24576], P('tp', 'sp')
All inputs are finite; a program needn't handle non-finite values.
Results may differ from a plain program's by a relative error of at most 0.009.
The roundings to bfloat16 on the way count: a program that leaves them out, or rounds other values in their place, can miss the bound.
Values may be sent and summed in bfloat16 or wider, within the bound.
A program may use at most 64 MiB of HBM per device.

v0:
```python
import math

import jax
import jax.numpy as jnp
from jax import lax
from jax.sharding import PartitionSpec as P

GRID_W = 64


ROPE_BASE = 10000.0
NORM_EPS = 1e-06


def in_blocks(x, dim, peers):
    shape = x.shape
    tiles = x.reshape(*shape[:dim], peers, shape[dim] // peers, *shape[dim + 1 :])
    return jnp.moveaxis(tiles, dim, 0)


def sum_at_owner(x, axis, dim):
    tiles = in_blocks(x, dim, lax.axis_size(axis))
    arrived = lax.all_to_all(tiles, axis, split_axis=0, concat_axis=0, tiled=True)
    return arrived.sum(axis=0)


def rotate(values, position):
    dim = values.shape[-1]
    half_dim = dim // 2
    inverse = ROPE_BASE ** (-jnp.arange(half_dim, dtype=jnp.float32) * (2.0 / dim))
    angles = position.astype(jnp.float32)[:, None] * inverse[None, :]
    cosine = jnp.cos(angles)[:, None, :]
    sine = jnp.sin(angles)[:, None, :]
    first_half = values[..., :half_dim]
    second_half = values[..., half_dim:]
    return jnp.concatenate(
        [first_half * cosine - second_half * sine, second_half * cosine + first_half * sine], -1
    )


def prepare(projected, gain_vec, grid_row, grid_col):
    values = projected.astype(jnp.float32)
    values = values * lax.rsqrt(jnp.mean(values * values, -1, keepdims=True) + NORM_EPS) * gain_vec
    split_at = values.shape[-1] // 2
    turned = jnp.concatenate(
        [rotate(values[..., :split_at], grid_row), rotate(values[..., split_at:], grid_col)], -1
    )
    return turned.astype(jnp.bfloat16)


def shards(tokens, w_query, w_key, w_value, w_output, query_gain, key_gain):
    head_dim = query_gain.shape[0]
    n_query = w_query.shape[1]
    n_key = w_key.shape[1]
    combined = jnp.concatenate([w_query, w_key, w_value], axis=1)
    projected = jnp.dot(tokens, combined, preferred_element_type=jnp.float32).astype(jnp.bfloat16)
    seq_rows = projected.shape[0]
    local_heads = n_query // head_dim
    local_kv = n_key // head_dim
    group_size = local_heads // local_kv
    positions = lax.axis_index("sp") * seq_rows + jnp.arange(seq_rows, dtype=jnp.int32)
    grid_row = positions // GRID_W
    grid_col = positions % GRID_W
    queries = prepare(
        projected[:, :n_query].reshape(seq_rows, local_heads, head_dim),
        query_gain,
        grid_row,
        grid_col,
    )
    key_rows = prepare(
        projected[:, n_query : n_query + n_key].reshape(seq_rows, local_kv, head_dim),
        key_gain,
        grid_row,
        grid_col,
    )
    key_value = jnp.concatenate(
        [key_rows.reshape(seq_rows, n_key), projected[:, n_query + n_key :]], axis=1
    )
    grouped = queries.reshape(seq_rows, local_kv, group_size, head_dim).transpose(1, 2, 0, 3)
    grouped = grouped.reshape(local_kv, group_size * seq_rows, head_dim)
    score_scale = head_dim ** (-0.5)
    initial = (
        jnp.full((local_kv, group_size * seq_rows), -1e30, jnp.float32),
        jnp.zeros((local_kv, group_size * seq_rows), jnp.float32),
        jnp.zeros((local_kv, group_size * seq_rows, head_dim), jnp.float32),
    )
    gathered = lax.all_gather(key_value, "sp", axis=0, tiled=True)
    piece_rows = gathered.shape[0]
    span_rows = math.gcd(piece_rows, 1024)
    pieces = gathered.reshape(piece_rows // span_rows, span_rows, 2, local_kv, head_dim)

    def update(state, block):
        running, totals, weighted = state
        key_block = block[:, 0]
        value_block = block[:, 1]
        scores = (
            jnp.einsum("kqd,skd->kqs", grouped, key_block, preferred_element_type=jnp.float32)
            * score_scale
        )
        new_max = jnp.maximum(running, jnp.max(scores, -1))
        shrink = jnp.exp(running - new_max)
        expos = jnp.exp(scores - new_max[..., None])
        totals = totals * shrink + jnp.sum(expos, -1)
        weighted = weighted * shrink[..., None] + jnp.einsum(
            "kqs,skd->kqd",
            expos.astype(jnp.bfloat16),
            value_block,
            preferred_element_type=jnp.float32,
        )
        return ((new_max, totals, weighted), None)

    result, unused = lax.scan(update, initial, pieces)
    running, totals, weighted = result
    attended = (weighted / totals[..., None]).astype(jnp.bfloat16)
    attended = (
        attended.reshape(local_kv, group_size, seq_rows, head_dim)
        .transpose(2, 0, 1, 3)
        .reshape(seq_rows, n_query)
    )
    log_sums = (running + jnp.log(totals)).reshape(local_heads, seq_rows)
    mixed_out = sum_at_owner(
        jnp.dot(attended, w_output, preferred_element_type=jnp.float32), "tp", 0
    ).astype(jnp.bfloat16)
    return (mixed_out, log_sums)


def solution(mesh):
    placed = (P("sp", None), P(None, "tp"), P(None, "tp"), P(None, "tp"), P("tp", None), P(), P())
    return jax.shard_map(
        shards,
        mesh=mesh,
        in_specs=placed,
        out_specs=(P(("sp", "tp"), None), P("tp", "sp")),
        check_vma=False,
    )
```

profile of v0, /device:TPU:1, one launch (start us, length us, event | category | flops | bytes accessed | tf_op | source)
XLA Modules:
  0.0 347.7 jit_solution(5974512695529500345)
XLA Ops:
  7.3 1.3 copy.35
  8.6 1.2 copy.36
  9.8 2.3 fusion.25
  14.2 91.3 %all-gather.2.cloned.1.call-done = bf16[24576,128]{1,0:T(8,128)(2,1)} async-done(((bf16[192,128]{1,0:T(8,128)(2,1)}), bf16[24576,128]{1,0:T(8,128)(2,1)}) %all-gather.2.cloned.1.call-update) | async-done | bytes 6291472 | tf_op jit(solution)/shard_map/all_gather | solution.py:87
  105.5 21.6 %reshape.404 = bf16[24,1024,2,1,64]{4,2,1,0,3:T(2,128)(2,1)} reshape(bf16[24576,128]{1,0:T(8,128)(2,1)} %all-gather.2.cloned.1.call-done) | data formatting | bytes 12582912 | tf_op jit(solution)/shard_map/reshape | solution.py:90
  127.1 26.0 %copy.41 = bf16[24,1024,2,1,64]{1,4,3,2,0:T(8,128)(2,1)} copy(bf16[24,1024,2,1,64]{4,2,1,0,3:T(2,128)(2,1)} %reshape.404) | data formatting | bytes 12582912
  153.0 160.7 %while.15 = (s32[]{:T(128)}, f32[1,768]{1,0:T(1,128)S(1)}, f32[1,768]{1,0:T(1,128)S(1)}, f32[1,768,64]{1,2,0:T(8,128)S(1)}, bf16[24,1024,2,1,64]{1,4,3,2,0:T(8,1...) while((s32[]{:T(128)}, f32[1,768]{1,0:T(1,128)S(1)}, ...), condition=%wide.region_5.6_spmd.clone, body=%wide.region_2.5_spmd.clone.sunk | while | flops 207770112 | bytes 23450752 | solution.py:112
  154.0 2.3 multiply_reduce_fusion.2
  156.3 2.7 fusion.70
  159.7 1.0 dynamic-slice_bitcast_fusion.2
  160.7 2.3 multiply_reduce_fusion.2
  163.0 2.7 fusion.70
  166.4 1.0 dynamic-slice_bitcast_fusion.2
  167.4 2.3 multiply_reduce_fusion.2
  169.7 2.7 fusion.70
  173.1 1.0 dynamic-slice_bitcast_fusion.2
  174.1 2.3 multiply_reduce_fusion.2
  176.4 2.7 fusion.70
  179.8 1.0 dynamic-slice_bitcast_fusion.2
  180.8 2.3 multiply_reduce_fusion.2
  183.1 2.7 fusion.70
  186.5 1.0 dynamic-slice_bitcast_fusion.2
  187.5 2.3 multiply_reduce_fusion.2
  189.8 2.7 fusion.70
  193.2 1.0 dynamic-slice_bitcast_fusion.2
  194.2 2.3 multiply_reduce_fusion.2
  196.5 2.7 fusion.70
  200.9 2.3 multiply_reduce_fusion.2
  203.2 2.7 fusion.70
  207.6 2.3 multiply_reduce_fusion.2
  209.9 2.7 fusion.70
  214.2 2.3 multiply_reduce_fusion.2
  216.6 2.7 fusion.70
  220.9 2.3 multiply_reduce_fusion.2
  223.3 2.7 fusion.70
  227.6 2.3 multiply_reduce_fusion.2
  229.9 2.7 fusion.70
  234.3 2.3 multiply_reduce_fusion.2
  236.6 2.7 fusion.70
  241.0 2.3 multiply_reduce_fusion.2
  243.3 2.7 fusion.70
  247.7 2.3 multiply_reduce_fusion.2
  250.0 2.7 fusion.70
  254.4 2.3 multiply_reduce_fusion.2
  256.7 2.7 fusion.70
  261.1 2.3 multiply_reduce_fusion.2
  263.4 2.7 fusion.70
  267.8 2.3 multiply_reduce_fusion.2
  270.1 2.7 fusion.70
  274.5 2.3 multiply_reduce_fusion.2
  276.8 2.7 fusion.70
  281.2 2.3 multiply_reduce_fusion.2
  283.5 2.7 fusion.70
  287.9 2.3 multiply_reduce_fusion.2
  290.2 2.7 fusion.70
  294.6 2.3 multiply_reduce_fusion.2
  296.9 2.7 fusion.70
  301.3 2.3 multiply_reduce_fusion.2
  303.6 2.7 fusion.70
  308.0 2.3 multiply_reduce_fusion.2
  310.3 2.7 fusion.70
  314.3 1.5 fusion.28
  315.8 4.0 %all-to-all-start = ((f32[4,48,2048]{2,1,0:T(8,128)}), f32[4,48,2048]{2,1,0:T(8,128)S(1)}, u32[]{:S(2)}, u32[]{:S(2)}) async-start(f32[4,48,2048]{2,1,0:T(8,128)} %fusion.28), calls=%async_computation | async-start | bytes 3145728 | tf_op jit(solution)/shard_map/all_to_all | solution.py:23
  320.5 19.6 %all-to-all-done = f32[4,48,2048]{2,1,0:T(8,128)S(1)} async-done(((f32[4,48,2048]{2,1,0:T(8,128)}), f32[4,48,2048]{2,1,0:T(8,128)S(1)}, u32[]{:S(2)}, u32[]{:S(2)}) %all-to-all-start) | async-done | bytes 1572896 | tf_op jit(solution)/shard_map/all_to_all | solution.py:23
  (198 shorter events, 38.1 us)
Async XLA Ops:
  7.2 307.1 %copy-start = (bf16[256,2048]{1,0:T(8,128)(2,1)S(1)}, bf16[256,2048]{1,0:T(8,128)(2,1)}, u32[]{:S(2)}) copy-start(bf16[256,2048]{1,0:T(8,128)(2,1)} %param.13) | copy-start | bytes 3145732
  7.2 98.3 %all-gather.2.cloned.1.call-start = ((), (), s32[]{:S(2)}) async-start(), calls=%async_computation.1 | async-start | bytes 6340608 | tf_op jit(solution)/shard_map/all_gather | solution.py:87
  9.8 2.4 copy-start.2
  9.8 4.1 %copy-start.3 = (f32[64]{0:T(128)S(1)}, f32[64]{0:T(128)}, u32[]{:S(2)}) copy-start(f32[64]{0:T(128)} %param.14) | copy-start | bytes 772
  156.3 2.8 copy-start.1
  163.0 2.8 copy-start.1
  169.7 2.8 copy-start.1
  176.4 2.8 copy-start.1
  183.1 2.8 copy-start.1
  189.7 2.8 copy-start.1
  196.4 2.8 copy-start.1
  203.1 2.8 copy-start.1
  209.8 2.8 copy-start.1
  216.5 2.8 copy-start.1
  223.2 2.8 copy-start.1
  229.9 2.8 copy-start.1
  236.6 2.8 copy-start.1
  243.3 2.8 copy-start.1
  250.0 2.8 copy-start.1
  256.7 2.8 copy-start.1
  263.4 2.8 copy-start.1
  270.1 2.8 copy-start.1
  276.8 2.8 copy-start.1
  283.5 2.8 copy-start.1
  290.2 2.8 copy-start.1
  296.9 2.8 copy-start.1
  303.6 2.8 copy-start.1
  310.3 2.8 copy-start.1
  315.8 24.2 %all-to-all-start = ((f32[4,48,2048]{2,1,0:T(8,128)}), f32[4,48,2048]{2,1,0:T(8,128)S(1)}, u32[]{:S(2)}, u32[]{:S(2)}) async-start(f32[4,48,2048]{2,1,0:T(8,128)} %fusion.28), calls=%async_computation | async-start | bytes 3145728 | tf_op jit(solution)/shard_map/all_to_all | solution.py:23
Sparse Core Ops, SparseCore 0:
  13.7 91.7 all-gather.1
where the time goes:
time: 350 us; the launch traced here: 348 us
  matrix products  124 us (35%)
  waiting for transfers between devices  111 us (32%)
  local copies, waits for them, and re-layouts  77.4 us (22%)
  other arithmetic  16.5 us (5%)
  between operations  14.2 us (4%)
  starting transfers between devices  4 us (1%)
    all_gather x1, waiting for transfers between devices, shards(): gathered = lax.all_gather(key_value, 'sp', axis=0, tiled=True)  91.3 us
    dot_general x24, matrix products, update(): jnp.einsum('kqs,skd->kqd', expos.astype(jnp.bfloat16), value_block, prefe...  65.3 us
    dot_general x24, matrix products, update(): jnp.einsum('kqd,skd->kqs', grouped, key_block, preferred_element_type=jnp...  54.7 us
    unnamed x10, local copies, waits for them, and re-layouts  28.7 us
    squeeze x24, local copies, waits for them, and re-layouts, shards(): result, unused = lax.scan(update, initial, pieces)  23.3 us
    reshape x1, local copies, waits for them, and re-layouts, shards(): gathered.reshape(piece_rows // span_rows, span_rows, 2, local_kv, head_dim)  21.6 us
    all_to_all x1, waiting for transfers between devices, sum_at_owner(): lax.all_to_all(tiles, axis, split_axis=0, concat_axis=0, tiled=True)  19.6 us
    reduce_sum x24, other arithmetic, update(): totals = totals * shrink + jnp.sum(expos, -1)  13.4 us
  transfers between devices with their start and end apart: 2, of which 2 were waited for; matrix products, arithmetic and copies ran while one was open for 0% of the time, Pallas kernels for 0%

commit v1 on v0

v1 whole, which is shorter than its diff:
```python
import numpy as np

import jax
import jax.numpy as jnp
from jax import lax
from jax.experimental import pallas as pl
from jax.experimental.pallas import tpu as pltpu
from jax.sharding import PartitionSpec as P

GRID_W = 64
ROPE_BASE = 10000.0
NORM_EPS = 1e-06
HEAD = 64
ROWS = 192
HALF_ROWS = ROWS // 2
RING = 8
CH = RING * HALF_ROWS
PIECE = CH // 2
ST = 256
QT = 256
NQ = 4 * ROWS
NJ = 2 * NQ // QT
D = 2048
TP = 4
OUT_ROWS = ROWS // TP
LOG2E = 1.4426950408889634
LN2 = 0.6931471805599453
FLOOR = -1e30
MESH = pl.DeviceIdType.MESH
OFFSETS = (0, 1, -1, 2, -2, 3, -3, 4)
STEPS = 7
POINT = {2: 0, 3: 1, 4: 2, 5: 4, 6: 5, 7: 6, 8: 8}


def kernel(
    tok_hbm, wq_hbm, wk_hbm, wv_hbm, wo_hbm, gq_ref, gk_ref, freq_ref,
    out_ref, lse_ref,
    tok, wq, wk, wv, kv, qbuf, wo, kk0, kk1, vt0, vt1, s0, s1, mb0, mb1,
    acc_p, acc_o, m_p, m_o, acc_r, m_r, att, att_in,
    load_sem, near_send, near_recv, far_send, far_recv, q_sem, o_send, o_recv,
    att_send, att_recv, w_send, w_recv,
):
    sp = lax.axis_index("sp")
    tp = lax.axis_index("tp")
    core = lax.rem(sp, 2)
    y = lax.rem(lax.div(sp, 2), RING)
    z = lax.div(sp, 2 * RING)

    def at(z_off, y_off):
        zz = lax.rem(z + (z_off + RING), RING)
        yy = lax.rem(y + (y_off + RING), RING)
        return ((zz * RING + yy) * 2 + core, tp)

    partner = (sp + 1 - 2 * core, tp)

    def peer(d):
        return (sp, lax.rem(tp + d, TP))

    barrier = pltpu.get_barrier_semaphore()
    greeted = [at(0, o) for o in OFFSETS[1:]] + [at(o, 0) for o in OFFSETS[1:]]
    greeted += [partner] + [peer(d) for d in (1, 2, 3)]
    for device in greeted:
        pl.semaphore_signal(barrier, inc=1, device_id=device, device_id_type=MESH)

    loads = [
        pltpu.make_async_copy(src, dst, load_sem.at[n])
        for n, (src, dst) in enumerate(((tok_hbm, tok), (wk_hbm, wk), (wv_hbm, wv), (wq_hbm, wq)))
    ]
    own_w = pltpu.make_async_copy(wo_hbm, wo.at[0], load_sem.at[4])
    for load in loads:
        load.start()

    lane = lax.broadcasted_iota(jnp.int32, (16, 2 * ROWS), 1)
    token = jnp.where(lane >= ROWS, lane - ROWS, lane)
    in_row = lax.shift_right_logical(token, 6)
    grid_row = sp * (ROWS // GRID_W) + in_row
    grid_col = token - in_row * GRID_W
    freq = freq_ref[...]
    row_angle = grid_row.astype(jnp.float32) * freq
    col_angle = grid_col.astype(jnp.float32) * freq
    row_cos, row_sin = jnp.cos(row_angle), jnp.sin(row_angle)
    col_cos, col_sin = jnp.cos(col_angle), jnp.sin(col_angle)

    eye = lax.broadcasted_iota(jnp.int32, (HEAD, HEAD), 0) == lax.broadcasted_iota(
        jnp.int32, (HEAD, HEAD), 1
    )

    def column(ref):
        return jnp.sum(
            jnp.where(eye, jnp.broadcast_to(ref[...], (HEAD, HEAD)), 0.0), axis=1, keepdims=True
        )

    def prepare(u, gain, width):
        scale = lax.rsqrt(jnp.mean(u * u, axis=0, keepdims=True) + NORM_EPS)
        u = u * scale * gain
        rc, rs = row_cos[:, :width], row_sin[:, :width]
        cc, cs = col_cos[:, :width], col_sin[:, :width]
        a, b, c, d = u[0:16], u[16:32], u[32:48], u[48:64]
        return jnp.concatenate(
            [a * rc - b * rs, b * rc + a * rs, c * cc - d * cs, d * cc + c * cs], axis=0
        )

    q_gain, k_gain = column(gq_ref), column(gk_ref)

    loads[0].wait()
    loads[1].wait()
    loads[2].wait()
    x = tok[...]
    key_raw = jnp.dot(x, wk[...], preferred_element_type=jnp.float32).astype(jnp.bfloat16)
    value_raw = jnp.dot(x, wv[...], preferred_element_type=jnp.float32).astype(jnp.bfloat16)
    both_raw = jnp.concatenate([key_raw, value_raw], axis=1).astype(jnp.float32)
    turned = both_raw.T
    key_t = prepare(turned[0:HEAD], k_gain, ROWS)
    block = jnp.concatenate([key_t, turned[HEAD:]], axis=0).T.astype(jnp.bfloat16)
    kv[0, 0, 0:HALF_ROWS, :] = block[0:HALF_ROWS]
    kv[1, 0, 0:HALF_ROWS, :] = block[HALF_ROWS:]

    loads[3].wait()
    own_w.start()
    query_raw = jnp.dot(x, wq[...], preferred_element_type=jnp.float32)
    query_raw = query_raw.astype(jnp.bfloat16).astype(jnp.float32)
    pairs = jnp.concatenate([query_raw[:, 0:128], query_raw[:, 128:256]], axis=0).T

    pl.semaphore_wait(barrier, len(greeted))

    near = []
    for n in range(2):
        for u in range(1, RING):
            there = at(0, OFFSETS[u]) if n == 0 else at(OFFSETS[u], 0)
            near.append((n, u, there))
    near.sort(key=lambda item: item[1])

    def near_copy(n, u, there):
        return pltpu.make_async_remote_copy(
            src_ref=kv.at[n, 0, pl.ds(0, HALF_ROWS)],
            dst_ref=kv.at[n, 0, pl.ds(u * HALF_ROWS, HALF_ROWS)],
            send_sem=near_send.at[n, u],
            recv_sem=near_recv.at[n, u],
            device_id=there,
            device_id_type=MESH,
        )

    for item in near:
        near_copy(*item).start()

    w_rows = pl.ds(core * 128, 128)

    def w_copy(step):
        if step == 0:
            src, dst, there = wo_hbm.at[w_rows], wo.at[3, w_rows], peer(1)
        elif step == 1:
            src, dst, there = wo_hbm.at[w_rows], wo.at[1, w_rows], peer(3)
        elif step == 2:
            rows = pl.ds(core * 128, 64)
            src, dst, there = wo.at[3, rows], wo.at[2, rows], peer(1)
        elif step == 3:
            rows = pl.ds(core * 128 + 64, 64)
            src, dst, there = wo.at[1, rows], wo.at[2, rows], peer(3)
        else:
            slot = (3, 1, 2)[step - 4]
            src = dst = wo.at[slot, w_rows]
            there = partner
        return pltpu.make_async_remote_copy(
            src_ref=src,
            dst_ref=dst,
            send_sem=w_send.at[step],
            recv_sem=w_recv.at[step],
            device_id=there,
            device_id_type=MESH,
        )

    w_copy(0).start()
    w_copy(1).start()

    q_turned = jnp.concatenate(
        [prepare(pairs[0:HEAD], q_gain, 2 * ROWS), prepare(pairs[HEAD:], q_gain, 2 * ROWS)], axis=1
    ).astype(jnp.bfloat16)
    scaled = q_turned.astype(jnp.float32) * jnp.float32(LOG2E / 8.0)
    high = scaled.astype(jnp.bfloat16)
    low = (scaled - high.astype(jnp.float32)).astype(jnp.bfloat16)
    qbuf[1, 0:HEAD, :] = high
    qbuf[1, HEAD:, :] = low

    acc_p[...] = jnp.zeros_like(acc_p)
    acc_o[...] = jnp.zeros_like(acc_o)
    m_p[...] = jnp.full_like(m_p, FLOOR)
    m_o[...] = jnp.full_like(m_o, FLOOR)
    ones = lax.broadcasted_iota(jnp.int32, (16, CH), 0) == 0
    for vt in (vt0, vt1):
        vt[HEAD:, :] = jnp.where(ones, 1.0, 0.0).astype(jnp.bfloat16)

    q_copy = pltpu.make_async_remote_copy(
        src_ref=qbuf.at[1],
        dst_ref=qbuf.at[0],
        send_sem=q_sem.at[0],
        recv_sem=q_sem.at[1],
        device_id=partner,
        device_id_type=MESH,
    )
    q_copy.start()

    def far_copy(n, way, k):
        m = k // 2
        piece = k % 2
        if way == 0:
            src, dst, off = max(0, 2 * m - 1), 2 * m + 1, 1
        else:
            src, dst, off = 2 * m, min(2 * m + 2, 7), -1
            if k == STEPS - 1:
                piece = 1
        rows = pl.ds(piece * PIECE, PIECE)
        return pltpu.make_async_remote_copy(
            src_ref=kv.at[n, src, rows],
            dst_ref=kv.at[n, dst, rows],
            send_sem=far_send.at[n, way, k],
            recv_sem=far_recv.at[n, way, k],
            device_id=at(off, 0) if n == 0 else at(0, off),
            device_id_type=MESH,
        )

    def far_step(k):
        for n in range(2):
            for way in range(2):
                if k >= 2:
                    back = k - 2
                    if way == 1 and k == STEPS - 1:
                        back = k - 1
                    elif way == 1 and k == STEPS:
                        back = k - 3
                    far_copy(n, way, back).wait_recv()
                if k < STEPS:
                    far_copy(n, way, k).start()

    for k in range(2):
        for item in near:
            if item[1] // 4 == k:
                near_copy(*item).wait_recv()
        far_step(k)

    q_copy.wait_recv()

    kk = (kk0, kk1)
    vts = (vt0, vt1)
    S = (s0, s1)
    mb = (mb0, mb1)
    accs = (acc_p, acc_o)
    ms = (m_p, m_o)

    def prep(n, slot):
        blk = kv[n, slot]
        k = blk[:, :HEAD]
        kk[n][...] = jnp.concatenate([k, k], axis=1)
        vts[n][0:HEAD, :] = blk.T[HEAD:]

    def colmax(v):
        return jnp.max(v.reshape(-1, 8, QT), axis=0)

    def finish_max(buf, m):
        mb[buf][...] = jnp.broadcast_to(jnp.max(m, axis=0, keepdims=True), (8, QT))

    def cols(j):
        return slice((j % 3) * QT, (j % 3 + 1) * QT)

    def score_strip(n, j, buf, r):
        s = jnp.dot(
            kk[n][r * ST : (r + 1) * ST, :],
            qbuf[j // 3, :, cols(j)],
            preferred_element_type=jnp.float32,
        )
        S[buf][r * ST : (r + 1) * ST, :] = s
        return colmax(s)

    def scores_only(n, j, buf):
        m = None
        for r in range(CH // ST):
            v = score_strip(n, j, buf, r)
            m = v if m is None else jnp.maximum(m, v)
        finish_max(buf, m)

    def both(na, ja, ba, nb, jb, bb):
        m_ref, acc = ms[jb // 3], accs[jb // 3]
        mo = m_ref[:, cols(jb)]
        mn = jnp.maximum(mo, mb[bb][...])
        f = jnp.exp2(mo - mn)
        m = None
        ot = None
        for r in range(CH // ST):
            v = score_strip(na, ja, ba, r)
            m = v if m is None else jnp.maximum(m, v)
            strip = S[bb][r * ST : (r + 1) * ST, :].reshape(ST // 8, 8, QT)
            p = jnp.exp2(strip - mn[None]).reshape(ST, QT).astype(jnp.bfloat16)
            o = jnp.dot(vts[nb][:, r * ST : (r + 1) * ST], p, preferred_element_type=jnp.float32)
            ot = o if ot is None else ot + o
        a = acc[:, cols(jb)].reshape(10, 8, QT)
        acc[:, cols(jb)] = (a * f[None]).reshape(80, QT) + ot
        m_ref[:, cols(jb)] = mn
        finish_max(ba, m)

    prep(0, 0)
    scores_only(0, 0, 0)

    def step(i, carry):
        for n in range(2):
            for k, point in POINT.items():
                if point % 2 == n:

                    @pl.when(i == point // 2)
                    def _():
                        far_step(k)

            if n == 1:

                @pl.when(i == 5)
                def _():
                    w_copy(0).wait_recv()
                    w_copy(1).wait_recv()
                    for s in (2, 3, 4, 5):
                        w_copy(s).start()

            prep(1 - n, i if n == 0 else jnp.minimum(i + 1, RING - 1))
            for j in range(NJ):
                buf = (n * NJ + j) % 2
                if j < NJ - 1:
                    both(n, j + 1, 1 - buf, n, j, buf)
                else:
                    both(1 - n, 0, 1 - buf, n, j, buf)
        return carry

    lax.fori_loop(0, RING, step, 0)

    def o_copy(n):
        src, dst = ((acc_p, acc_r), (m_p, m_r))[n]
        return pltpu.make_async_remote_copy(
            src_ref=src,
            dst_ref=dst,
            send_sem=o_send.at[n],
            recv_sem=o_recv.at[n],
            device_id=partner,
            device_id_type=MESH,
        )

    o_copy(0).start()
    o_copy(1).start()
    w_copy(2).wait_recv()
    w_copy(3).wait_recv()
    w_copy(6).start()
    own_w.wait()
    o_copy(0).wait_recv()
    o_copy(1).wait_recv()

    m_all = jnp.maximum(m_o[...], m_r[...])
    f_o = jnp.exp2(m_o[...] - m_all)
    f_r = jnp.exp2(m_r[...] - m_all)
    total = (
        acc_o[...].reshape(10, 8, NQ) * f_o[None] + acc_r[...].reshape(10, 8, NQ) * f_r[None]
    ).reshape(80, NQ)
    weight_sum = total[HEAD : HEAD + 1]
    attended = total[0:HEAD] / weight_sum
    lse = (m_all[0:1] + jnp.log2(weight_sum)) * LN2
    for place, head in enumerate((0, 2, 1, 3)):
        lse_ref[head : head + 1, :] = lse[:, place * ROWS : (place + 1) * ROWS]
    mixed = jnp.concatenate([attended[:, : 2 * ROWS], attended[:, 2 * ROWS :]], axis=0).T
    mixed = jnp.concatenate([mixed[0:ROWS], mixed[ROWS:]], axis=1).astype(jnp.bfloat16)
    att[...] = mixed.reshape(TP, OUT_ROWS, 4 * HEAD)

    def att_copy(d):
        return pltpu.make_async_remote_copy(
            src_ref=att.at[lax.rem(tp + d, TP)],
            dst_ref=att_in.at[TP - d],
            send_sem=att_send.at[d],
            recv_sem=att_recv.at[TP - d],
            device_id=peer(d),
            device_id_type=MESH,
        )

    for d in (2, 1, 3):
        att_copy(d).start()
    result = jnp.dot(att[tp], wo[0], preferred_element_type=jnp.float32)
    for s in (4, 5, 6):
        w_copy(s).wait_recv()
    for d in (1, 3, 2):
        att_copy(TP - d).wait_recv()
        result = result + jnp.dot(att_in[d], wo[d], preferred_element_type=jnp.float32)
    out_ref[...] = result.astype(jnp.bfloat16)

    for item in near:
        near_copy(*item).wait_send()
    for n in range(2):
        for way in range(2):
            for k in range(STEPS):
                far_copy(n, way, k).wait_send()
        o_copy(n).wait_send()
    q_copy.wait_send()
    for d in (1, 2, 3):
        att_copy(d).wait_send()
    for s in range(7):
        w_copy(s).wait_send()


def shards(tokens, w_query, w_key, w_value, w_output, query_gain, key_gain):
    inverse = np.float32(ROPE_BASE) ** (-np.arange(16, dtype=np.float32) * np.float32(2.0 / 32))
    freq = jnp.asarray(np.broadcast_to(inverse.astype(np.float32)[:, None], (16, 2 * ROWS)))
    vmem = pltpu.VMEM
    bf16, f32 = jnp.bfloat16, jnp.float32
    dma = pltpu.SemaphoreType.DMA
    hbm = pl.BlockSpec(memory_space=pl.ANY)
    local = pl.BlockSpec(memory_space=vmem)
    return pl.pallas_call(
        kernel,
        out_shape=(
            jax.ShapeDtypeStruct((OUT_ROWS, D), bf16),
            jax.ShapeDtypeStruct((4, ROWS), f32),
        ),
        in_specs=[hbm] * 5 + [local] * 3,
        out_specs=(local, local),
        scratch_shapes=[
            vmem((ROWS, D), bf16),
            vmem((D, 4 * HEAD), bf16),
            vmem((D, HEAD), bf16),
            vmem((D, HEAD), bf16),
            vmem((2, RING, CH, 2 * HEAD), bf16),
            vmem((2, 2 * HEAD, NQ), bf16),
            vmem((TP, 4 * HEAD, D), bf16),
            vmem((CH, 2 * HEAD), bf16),
            vmem((CH, 2 * HEAD), bf16),
            vmem((80, CH), bf16),
            vmem((80, CH), bf16),
            vmem((CH, QT), f32),
            vmem((CH, QT), f32),
            vmem((8, QT), f32),
            vmem((8, QT), f32),
            vmem((80, NQ), f32),
            vmem((80, NQ), f32),
            vmem((8, NQ), f32),
            vmem((8, NQ), f32),
            vmem((80, NQ), f32),
            vmem((8, NQ), f32),
            vmem((TP, OUT_ROWS, 4 * HEAD), bf16),
            vmem((TP, OUT_ROWS, 4 * HEAD), bf16),
            dma((5,)),
            dma((2, RING)),
            dma((2, RING)),
            dma((2, 2, STEPS)),
            dma((2, 2, STEPS)),
            dma((2,)),
            dma((2,)),
            dma((2,)),
            dma((TP,)),
            dma((TP,)),
            dma((7,)),
            dma((7,)),
        ],
        compiler_params=pltpu.CompilerParams(
            collective_id=0, has_side_effects=True, vmem_limit_bytes=58 << 20
        ),
        name="layer",
    )(
        tokens, w_query, w_key, w_value, w_output,
        query_gain.reshape(1, HEAD), key_gain.reshape(1, HEAD), freq,
    )


def solution(mesh):
    placed = (P("sp", None), P(None, "tp"), P(None, "tp"), P(None, "tp"), P("tp", None), P(), P())
    return jax.shard_map(
        shards,
        mesh=mesh,
        in_specs=placed,
        out_specs=(P(("sp", "tp"), None), P("tp", "sp")),
        check_vma=False,
    )
```

time: 350 us -> 68.8 us (0.20)
  matrix products: 124 us -> 0 us
  waiting for transfers between devices: 111 us -> 0 us
  local copies, waits for them, and re-layouts: 77.4 us -> 5.89 us
  Pallas kernels: 0 us -> 62.1 us
  other arithmetic: 16.5 us -> 0 us
  between operations: 14.2 us -> 0.66 us
  starting transfers between devices: 4 us -> 0 us
    dot_general x50 -> x0, matrix products: 124 us -> none  [the longest x24 65.3 us: update(): jnp.einsum('kqs,skd->kqd', expos.astype(jnp.bfloat16), value_block, prefe...]
    all_gather x1 -> x0, waiting for transfers between devices: 91.3 us -> none  [shards(): gathered = lax.all_gather(key_value, 'sp', axis=0, tiled=True)]
    pallas_call x0 -> x1, Pallas kernels: none -> 62.1 us  [shards(): pl.pallas_call(kernel, out_shape=(jax.ShapeDtypeStruct((OUT_ROWS, D), bf1...]
    unnamed x10, local copies, waits for them, and re-layouts: 28.7 us -> 5.21 us
    squeeze x24 -> x0, local copies, waits for them, and re-layouts: 23.3 us -> none  [shards(): result, unused = lax.scan(update, initial, pieces)]
    reshape x4 -> x0, local copies, waits for them, and re-layouts: 22.6 us -> none  [the longest x1 21.6 us: shards(): gathered.reshape(piece_rows // span_rows, span_rows, 2, local_kv, head_dim)]
    all_to_all x1 -> x0, waiting for transfers between devices: 19.6 us -> none  [sum_at_owner(): lax.all_to_all(tiles, axis, split_axis=0, concat_axis=0, tiled=True)]
    reduce_sum x27 -> x0, other arithmetic: 14.3 us -> none  [the longest x24 13.4 us: update(): totals = totals * shrink + jnp.sum(expos, -1)]
  transfers between devices with their start and end apart: 2 -> 0, of which waited for: 2 -> 0; matrix products, arithmetic and copies ran while one was open for 0% -> 0% of each run, Pallas kernels for 0% -> 0%
where the time goes in v1:
time: 68.8 us; the launch traced here: 68.6 us
  Pallas kernels  62.1 us (90%)
  local copies, waits for them, and re-layouts  5.89 us (9%)
    pallas_call x1, Pallas kernels, shards(): pl.pallas_call(kernel, out_shape=(jax.ShapeDtypeStruct((OUT_ROWS, D), bf1...  62.1 us
    unnamed x10, local copies, waits for them, and re-layouts  5.21 us

profile of v1, /device:TPU:1, one launch (start us, length us, event | category | flops | bytes accessed | tf_op | source)
XLA Modules:
  0.0 68.6 jit_solution(17236649941427179125)
XLA Ops:
  0.6 0.0 copy-start
  0.6 2.0 %copy.10.wk_hbm = bf16[2048,64]{1,0:T(8,128)(2,1)} copy(bf16[2048,64]{0,1:T(8,128)(2,1)} %param.10) | data formatting | bytes 524288 | tf_op args[2]
  2.6 0.0 copy-done
  2.6 0.0 copy-start.2
  2.6 1.0 %copy.11.wv_hbm = bf16[2048,64]{1,0:T(8,128)(2,1)} copy(bf16[2048,64]{0,1:T(8,128)(2,1)S(1)} %copy-done) | data formatting | bytes 524288 | tf_op args[3]
  3.6 0.0 copy-done.2
  3.6 0.7 jit_solution_.3.freq_ref
  4.3 62.1 %layer.1 = (bf16[48,2048]{1,0:T(8,128)(2,1)}, f32[4,192]{1,0:T(4,128)}) custom-call(bf16[192,2048]{1,0:T(8,128)(2,1)} %tok_hbm.1, bf16[2048,256]{1,0:T(8,128)(2,1)} %wq_hbm.1, bf16[2048,64]{1,0:T(8,128)(2,1)} %copy.10.wk_hbm, bf16[2048,64]{1,0:T(8,128)(2,1)} %copy.11.wv_hbm, bf16[256,2048]{1,0:T(8,128)(2,1)} %wo_hbm.1, f32[1,64]{1,0:T(1,128)} %bitcast.2, ...), custom_call_target="tpu_custom_call" | custom-call | tf_op jit(solution)/shard_map/layer/pallas_call | solution.py:408
  66.4 0.0 copy-start.1
  66.4 1.6 %copy.14 = bf16[48,2048]{1,0:T(8,128)(2,1)} copy(bf16[48,2048]{1,0:T(8,128)(2,1)} %get-tuple-element.4) | data formatting | bytes 393216
  68.0 0.0 copy-done.1
  68.0 0.6 copy.15
Async XLA Ops:
  0.6 2.0 %copy-start = (bf16[2048,64]{0,1:T(8,128)(2,1)S(1)}, bf16[2048,64]{0,1:T(8,128)(2,1)}, u32[]{:S(2)}) copy-start(bf16[2048,64]{0,1:T(8,128)(2,1)} %param.11) | copy-start | bytes 786436
  2.6 1.0 %copy-start.2 = (f32[16]{0:T(128)S(1)}, f32[16]{0:T(128)}, u32[]{:S(2)}) copy-start(f32[16]{0:T(128)} %constant.2.clone) | copy-start | bytes 196
  66.4 1.6 %copy-start.1 = (f32[4,192]{1,0:T(4,128)S(1)}, f32[4,192]{1,0:T(4,128)}, u32[]{:S(2)}) copy-start(f32[4,192]{1,0:T(4,128)} %get-tuple-element.5) | copy-start | bytes 9220

commit v2 on v1

--- a/solution.py
+++ b/solution.py
@@ -14,9 +14,10 @@
 ROWS = 192
 HALF_ROWS = ROWS // 2
 RING = 8
-CH = RING * HALF_ROWS
-PIECE = CH // 2
-ST = 256
+CH_UNITS = 16
+CH = CH_UNITS * HALF_ROWS
+W_POINT = 16
+ST = 768
 QT = 256
 NQ = 4 * ROWS
 NJ = 2 * NQ // QT
@@ -26,18 +27,63 @@
 LOG2E = 1.4426950408889634
 LN2 = 0.6931471805599453
 FLOOR = -1e30
+FREQUENCIES = [float(f) for f in np.float32(ROPE_BASE) ** (-np.arange(16, dtype=np.float32) * np.float32(2.0 / 32))]
 MESH = pl.DeviceIdType.MESH
-OFFSETS = (0, 1, -1, 2, -2, 3, -3, 4)
-STEPS = 7
-POINT = {2: 0, 3: 1, 4: 2, 5: 4, 6: 5, 7: 6, 8: 8}
+UNITS = 2 * RING * RING
+CHUNKS = UNITS * HALF_ROWS // CH
+CLASSES = ((0,), (1, -1), (2, -2), (3, -3), (4,))
+
+
+def gather_plan():
+    rows = (0, 1, -1, 2, -2, 3, -3, 4)
+    order = []
+    for row in rows:
+        for c, offsets in enumerate(CLASSES):
+            for n in range(2):
+                order.append((abs(row) + (c > 0), c, n, rows.index(row), offsets))
+    order.sort()
+    slot = {}
+    for _, _, n, r, offsets in order:
+        for o in offsets:
+            slot[n, rows[r], o] = len(slot)
+    copies = []
+    for n in range(2):
+        for c in range(1, len(CLASSES)):
+            for o in CLASSES[c]:
+                copies.append(((0, 0), (1, c), (n, 0, 0), (n, 0, o), 1, n, True, o))
+        for c, offsets in enumerate(CLASSES):
+            for way in (1, -1):
+                for step in range(4):
+                    row, to = way * step, way * (step + 1)
+                    part = offsets
+                    if step == 3:
+                        to = 4
+                        if len(offsets) == 2:
+                            part = offsets[:1] if way == 1 else offsets[1:]
+                        elif (way == 1) != ((n == 0) == (c == 0)):
+                            part = ()
+                    if part:
+                        copies.append(
+                            ((step + (c > 0), c), (step + 1 + (c > 0), c), (n, row, part[0]), (n, to, part[0]), len(part), n, False, way)
+                        )
+    copies.sort(key=lambda copy: (copy[0], copy[6]))
+    return slot, copies
+
+
+SLOT, COPIES = gather_plan()
+GROUPS = sorted({copy[1] for copy in COPIES})
+POINT = {
+    (1, 0): -1, (1, 1): -1, (1, 2): -1, (1, 3): -1, (1, 4): 2, (2, 0): 2, (2, 1): 2, (2, 2): 3, (2, 3): 5, (2, 4): 6, (3, 0): 6, (3, 1): 7, (3, 2): 8, (3, 3): 10, (3, 4): 11, (4, 0): 11, (4, 1): 12, (4, 2): 13, (4, 3): 14, (4, 4): 15, (5, 1): 16, (5, 2): 17, (5, 3): 18, (5, 4): 19,
+}
+THIRDS = (0, 2, 4)
 
 
 def kernel(
-    tok_hbm, wq_hbm, wk_hbm, wv_hbm, wo_hbm, gq_ref, gk_ref, freq_ref,
+    tok_hbm, wq_hbm, wk_hbm, wv_hbm, wo_hbm, gq_ref, gk_ref,
     out_ref, lse_ref,
     tok, wq, wk, wv, kv, qbuf, wo, kk0, kk1, vt0, vt1, s0, s1, mb0, mb1,
     acc_p, acc_o, m_p, m_o, acc_r, m_r, att, att_in,
-    load_sem, near_send, near_recv, far_send, far_recv, q_sem, o_send, o_recv,
+    load_sem, kv_send, kv_recv, q_sem, o_send, o_recv,
     att_send, att_recv, w_send, w_recv,
 ):
     sp = lax.axis_index("sp")
@@ -57,7 +103,7 @@
         return (sp, lax.rem(tp + d, TP))
 
     barrier = pltpu.get_barrier_semaphore()
-    greeted = [at(0, o) for o in OFFSETS[1:]] + [at(o, 0) for o in OFFSETS[1:]]
+    greeted = [at(0, o) for c in CLASSES[1:] for o in c] + [at(o, 0) for c in CLASSES[1:] for o in c]
     greeted += [partner] + [peer(d) for d in (1, 2, 3)]
     for device in greeted:
         pl.semaphore_signal(barrier, inc=1, device_id=device, device_id_type=MESH)
@@ -75,7 +121,11 @@
     in_row = lax.shift_right_logical(token, 6)
     grid_row = sp * (ROWS // GRID_W) + in_row
     grid_col = token - in_row * GRID_W
-    freq = freq_ref[...]
+    channel = lax.broadcasted_iota(jnp.int32, (16, 128), 0)
+    freq = jnp.zeros((16, 128), jnp.float32)
+    for n in range(16):
+        freq = jnp.where(channel == n, FREQUENCIES[n], freq)
+    freq = jnp.concatenate([freq, freq, freq], axis=1)
     row_angle = grid_row.astype(jnp.float32) * freq
     col_angle = grid_col.astype(jnp.float32) * freq
     row_cos, row_sin = jnp.cos(row_angle), jnp.sin(row_angle)
@@ -102,46 +152,50 @@
 
     q_gain, k_gain = column(gq_ref), column(gk_ref)
 
+    def project(w, x):
+        return lax.dot_general(w, x, (((1,), (1,)), ((), ())), preferred_element_type=jnp.float32)
+
+
     loads[0].wait()
     loads[1].wait()
     loads[2].wait()
     x = tok[...]
-    key_raw = jnp.dot(x, wk[...], preferred_element_type=jnp.float32).astype(jnp.bfloat16)
-    value_raw = jnp.dot(x, wv[...], preferred_element_type=jnp.float32).astype(jnp.bfloat16)
-    both_raw = jnp.concatenate([key_raw, value_raw], axis=1).astype(jnp.float32)
-    turned = both_raw.T
-    key_t = prepare(turned[0:HEAD], k_gain, ROWS)
-    block = jnp.concatenate([key_t, turned[HEAD:]], axis=0).T.astype(jnp.bfloat16)
-    kv[0, 0, 0:HALF_ROWS, :] = block[0:HALF_ROWS]
-    kv[1, 0, 0:HALF_ROWS, :] = block[HALF_ROWS:]
+    key_raw = project(wk[...], x).astype(jnp.bfloat16).astype(jnp.float32)
+    value_raw = project(wv[...], x).astype(jnp.bfloat16).astype(jnp.float32)
+    key_t = prepare(key_raw, k_gain, ROWS)
+    block = jnp.concatenate([key_t, value_raw], axis=0).T.astype(jnp.bfloat16)
+    kv[SLOT[0, 0, 0]] = block[0:HALF_ROWS]
+    kv[SLOT[1, 0, 0]] = block[HALF_ROWS:]
+
+    pl.semaphore_wait(barrier, len(greeted))
+
+    def kv_copy(m):
+        _, _, source, target, units, n, near, places = COPIES[m]
+        along_y = (n == 0) == near
+        return pltpu.make_async_remote_copy(
+            src_ref=kv.at[pl.ds(SLOT[source], units)],
+            dst_ref=kv.at[pl.ds(SLOT[target], units)],
+            send_sem=kv_send.at[m],
+            recv_sem=kv_recv.at[m],
+            device_id=at(0, places) if along_y else at(places, 0),
+            device_id_type=MESH,
+        )
+
+    def forward(group):
+        for m, copy in enumerate(COPIES):
+            if copy[1] == group:
+                kv_copy(m).wait_recv()
+        for m, copy in enumerate(COPIES):
+            if copy[0] == group:
+                kv_copy(m).start()
+
+    forward((0, 0))
 
     loads[3].wait()
     own_w.start()
     query_raw = jnp.dot(x, wq[...], preferred_element_type=jnp.float32)
     query_raw = query_raw.astype(jnp.bfloat16).astype(jnp.float32)
     pairs = jnp.concatenate([query_raw[:, 0:128], query_raw[:, 128:256]], axis=0).T
-
-    pl.semaphore_wait(barrier, len(greeted))
-
-    near = []
-    for n in range(2):
-        for u in range(1, RING):
-            there = at(0, OFFSETS[u]) if n == 0 else at(OFFSETS[u], 0)
-            near.append((n, u, there))
-    near.sort(key=lambda item: item[1])
-
-    def near_copy(n, u, there):
-        return pltpu.make_async_remote_copy(
-            src_ref=kv.at[n, 0, pl.ds(0, HALF_ROWS)],
-            dst_ref=kv.at[n, 0, pl.ds(u * HALF_ROWS, HALF_ROWS)],
-            send_sem=near_send.at[n, u],
-            recv_sem=near_recv.at[n, u],
-            device_id=there,
-            device_id_type=MESH,
-        )
-
-    for item in near:
-        near_copy(*item).start()
 
     w_rows = pl.ds(core * 128, 128)
 
@@ -199,43 +253,9 @@
     )
     q_copy.start()
 
-    def far_copy(n, way, k):
-        m = k // 2
-        piece = k % 2
-        if way == 0:
-            src, dst, off = max(0, 2 * m - 1), 2 * m + 1, 1
-        else:
-            src, dst, off = 2 * m, min(2 * m + 2, 7), -1
-            if k == STEPS - 1:
-                piece = 1
-        rows = pl.ds(piece * PIECE, PIECE)
-        return pltpu.make_async_remote_copy(
-            src_ref=kv.at[n, src, rows],
-            dst_ref=kv.at[n, dst, rows],
-            send_sem=far_send.at[n, way, k],
-            recv_sem=far_recv.at[n, way, k],
-            device_id=at(off, 0) if n == 0 else at(0, off),
-            device_id_type=MESH,
-        )
-
-    def far_step(k):
-        for n in range(2):
-            for way in range(2):
-                if k >= 2:
-                    back = k - 2
-                    if way == 1 and k == STEPS - 1:
-                        back = k - 1
-                    elif way == 1 and k == STEPS:
-                        back = k - 3
-                    far_copy(n, way, back).wait_recv()
-                if k < STEPS:
-                    far_copy(n, way, k).start()
-
-    for k in range(2):
-        for item in near:
-            if item[1] // 4 == k:
-                near_copy(*item).wait_recv()
-        far_step(k)
+    for group in GROUPS:
+        if POINT[group] < 0:
+            forward(group)
 
     q_copy.wait_recv()
 
@@ -246,8 +266,8 @@
     accs = (acc_p, acc_o)
     ms = (m_p, m_o)
 
-    def prep(n, slot):
-        blk = kv[n, slot]
+    def prep(n, c):
+        blk = kv[pl.ds(pl.multiple_of(c * CH_UNITS, CH_UNITS), CH_UNITS)].reshape(CH, 2 * HEAD)
         k = blk[:, :HEAD]
         kk[n][...] = jnp.concatenate([k, k], axis=1)
         vts[n][0:HEAD, :] = blk.T[HEAD:]
@@ -296,38 +316,6 @@
         m_ref[:, cols(jb)] = mn
         finish_max(ba, m)
 
-    prep(0, 0)
-    scores_only(0, 0, 0)
-
-    def step(i, carry):
-        for n in range(2):
-            for k, point in POINT.items():
-                if point % 2 == n:
-
-                    @pl.when(i == point // 2)
-                    def _():
-                        far_step(k)
-
-            if n == 1:
-
-                @pl.when(i == 5)
-                def _():
-                    w_copy(0).wait_recv()
-                    w_copy(1).wait_recv()
-                    for s in (2, 3, 4, 5):
-                        w_copy(s).start()
-
-            prep(1 - n, i if n == 0 else jnp.minimum(i + 1, RING - 1))
-            for j in range(NJ):
-                buf = (n * NJ + j) % 2
-                if j < NJ - 1:
-                    both(n, j + 1, 1 - buf, n, j, buf)
-                else:
-                    both(1 - n, 0, 1 - buf, n, j, buf)
-        return carry
-
-    lax.fori_loop(0, RING, step, 0)
-
     def o_copy(n):
         src, dst = ((acc_p, acc_r), (m_p, m_r))[n]
         return pltpu.make_async_remote_copy(
@@ -339,8 +327,48 @@
             device_id_type=MESH,
         )
 
-    o_copy(0).start()
-    o_copy(1).start()
+    prep(0, 0)
+    scores_only(0, 0, 0)
+
+    def step(i, carry):
+        for n in range(2):
+            for j in range(NJ):
+                buf = (n * NJ + j) % 2
+                if j in THIRDS:
+                    third = THIRDS.index(j)
+                    for group in GROUPS:
+                        if POINT[group] >= 0 and POINT[group] % 6 == 3 * n + third:
+
+                            @pl.when(i == POINT[group] // 6)
+                            def _():
+                                forward(group)
+
+                    if W_POINT % 6 == 3 * n + third:
+
+                        @pl.when(i == W_POINT // 6)
+                        def _():
+                            w_copy(0).wait_recv()
+                            w_copy(1).wait_recv()
+                            for s in (2, 3, 4, 5):
+                                w_copy(s).start()
+
+                    if n == 1 and third == 2:
+
+                        @pl.when(i == CHUNKS // 2 - 1)
+                        def _():
+                            o_copy(0).start()
+                            o_copy(1).start()
+
+                    if third == 2:
+                        prep(1 - n, jnp.minimum(2 * i + n + 1, CHUNKS - 1))
+                if j < NJ - 1:
+                    both(n, j + 1, 1 - buf, n, j, buf)
+                else:
+                    both(1 - n, 0, 1 - buf, n, j, buf)
+        return carry
+
+    lax.fori_loop(0, CHUNKS // 2, step, 0)
+
     w_copy(2).wait_recv()
     w_copy(3).wait_recv()
     w_copy(6).start()
@@ -383,12 +411,9 @@
         result = result + jnp.dot(att_in[d], wo[d], preferred_element_type=jnp.float32)
     out_ref[...] = result.astype(jnp.bfloat16)
 
-    for item in near:
-        near_copy(*item).wait_send()
+    for m in range(len(COPIES)):
+        kv_copy(m).wait_send()
     for n in range(2):
-        for way in range(2):
-            for k in range(STEPS):
-                far_copy(n, way, k).wait_send()
         o_copy(n).wait_send()
     q_copy.wait_send()
     for d in (1, 2, 3):
@@ -398,8 +423,6 @@
 
 
 def shards(tokens, w_query, w_key, w_value, w_output, query_gain, key_gain):
-    inverse = np.float32(ROPE_BASE) ** (-np.arange(16, dtype=np.float32) * np.float32(2.0 / 32))
-    freq = jnp.asarray(np.broadcast_to(inverse.astype(np.float32)[:, None], (16, 2 * ROWS)))
     vmem = pltpu.VMEM
     bf16, f32 = jnp.bfloat16, jnp.float32
     dma = pltpu.SemaphoreType.DMA
@@ -411,14 +434,14 @@
             jax.ShapeDtypeStruct((OUT_ROWS, D), bf16),
             jax.ShapeDtypeStruct((4, ROWS), f32),
         ),
-        in_specs=[hbm] * 5 + [local] * 3,
+        in_specs=[hbm] * 5 + [local] * 2,
         out_specs=(local, local),
         scratch_shapes=[
             vmem((ROWS, D), bf16),
             vmem((D, 4 * HEAD), bf16),
-            vmem((D, HEAD), bf16),
-            vmem((D, HEAD), bf16),
-            vmem((2, RING, CH, 2 * HEAD), bf16),
+            vmem((HEAD, D), bf16),
+            vmem((HEAD, D), bf16),
+            vmem((UNITS, HALF_ROWS, 2 * HEAD), bf16),
             vmem((2, 2 * HEAD, NQ), bf16),
             vmem((TP, 4 * HEAD, D), bf16),
             vmem((CH, 2 * HEAD), bf16),
@@ -438,10 +461,8 @@
             vmem((TP, OUT_ROWS, 4 * HEAD), bf16),
             vmem((TP, OUT_ROWS, 4 * HEAD), bf16),
             dma((5,)),
-            dma((2, RING)),
-            dma((2, RING)),
-            dma((2, 2, STEPS)),
-            dma((2, 2, STEPS)),
+            dma((len(COPIES),)),
+            dma((len(COPIES),)),
             dma((2,)),
             dma((2,)),
             dma((2,)),
@@ -455,8 +476,8 @@
         ),
         name="layer",
     )(
-        tokens, w_query, w_key, w_value, w_output,
-        query_gain.reshape(1, HEAD), key_gain.reshape(1, HEAD), freq,
+        tokens, w_query, w_key.T, w_value.T, w_output,
+        query_gain.reshape(1, HEAD), key_gain.reshape(1, HEAD),
     )
 
 

time: 68.8 us -> 57.4 us (0.83)
  Pallas kernels: 62.1 us -> 54.4 us
  local copies, waits for them, and re-layouts: 5.89 us -> 2.21 us
    pallas_call x1, Pallas kernels: 62.1 us -> 54.4 us  [shards(): pl.pallas_call(kernel, out_shape=(jax.ShapeDtypeStruct((OUT_ROWS, D), bf1...]
    unnamed x10 -> x4, local copies, waits for them, and re-layouts: 5.21 us -> 2.21 us
where the time goes in v2:
time: 57.4 us; the launch traced here: 57.2 us
  Pallas kernels  54.4 us (95%)
  local copies, waits for them, and re-layouts  2.21 us (4%)
  between operations  0.65 us (1%)
    pallas_call x1, Pallas kernels, shards(): pl.pallas_call(kernel, out_shape=(jax.ShapeDtypeStruct((OUT_ROWS, D), bf1...  54.4 us
    unnamed x4, local copies, waits for them, and re-layouts  2.21 us

profile of v2, /device:TPU:1, one launch (start us, length us, event | category | flops | bytes accessed | tf_op | source)
XLA Modules:
  0.0 57.2 jit_solution(16589972176141582268)
XLA Ops:
  0.6 54.4 %layer.1 = (bf16[48,2048]{1,0:T(8,128)(2,1)}, f32[4,192]{1,0:T(4,128)}) custom-call(bf16[192,2048]{1,0:T(8,128)(2,1)} %tok_hbm.1, bf16[2048,256]{1,0:T(8,128)(2,1)} %wq_hbm.1, bf16[64,2048]{1,0:T(8,128)(2,1)} %bitcast.4, bf16[64,2048]{1,0:T(8,128)(2,1)} %bitcast.5, bf16[256,2048]{1,0:T(8,128)(2,1)} %wo_hbm.1, f32[1,64]{1,0:T(1,128)} %bitcast.6, f32[1,64]{1,0:T(1,128)} %bitcast.7), custom_call_target="tpu_custom_call" | custom-call | tf_op jit(solution)/shard_map/layer/pallas_call | solution.py:431
  55.0 0.0 copy-start
  55.0 1.6 %copy.11 = bf16[48,2048]{1,0:T(8,128)(2,1)} copy(bf16[48,2048]{1,0:T(8,128)(2,1)} %get-tuple-element.4) | data formatting | bytes 393216
  56.6 0.0 copy-done
  56.6 0.6 %copy.12 = f32[4,192]{1,0:T(4,128)} copy(f32[4,192]{1,0:T(4,128)S(1)} %copy-done) | data formatting | bytes 6144
Async XLA Ops:
  55.0 1.6 %copy-start = (f32[4,192]{1,0:T(4,128)S(1)}, f32[4,192]{1,0:T(4,128)}, u32[]{:S(2)}) copy-start(f32[4,192]{1,0:T(4,128)} %get-tuple-element.5) | copy-start | bytes 9220

commit v3 on v2

--- a/solution.py
+++ b/solution.py
@@ -73,7 +73,7 @@
 SLOT, COPIES = gather_plan()
 GROUPS = sorted({copy[1] for copy in COPIES})
 POINT = {
-    (1, 0): -1, (1, 1): -1, (1, 2): -1, (1, 3): -1, (1, 4): 2, (2, 0): 2, (2, 1): 2, (2, 2): 3, (2, 3): 5, (2, 4): 6, (3, 0): 6, (3, 1): 7, (3, 2): 8, (3, 3): 10, (3, 4): 11, (4, 0): 11, (4, 1): 12, (4, 2): 13, (4, 3): 14, (4, 4): 15, (5, 1): 16, (5, 2): 17, (5, 3): 18, (5, 4): 19,
+    (1, 0): -1, (1, 1): -1, (1, 2): -1, (1, 3): -1, (1, 4): 2, (2, 0): 2, (2, 1): 2, (2, 2): 4, (2, 3): 5, (2, 4): 6, (3, 0): 6, (3, 1): 8, (3, 2): 9, (3, 3): 11, (3, 4): 12, (4, 0): 12, (4, 1): 13, (4, 2): 14, (4, 3): 15, (4, 4): 16, (5, 1): 17, (5, 2): 18, (5, 3): 19, (5, 4): 20,
 }
 THIRDS = (0, 2, 4)
 
@@ -422,13 +422,18 @@
         w_copy(s).wait_send()
 
 
+def hand_over(mixed_ref, log_ref, mixed_out_ref, log_out_ref):
+    mixed_out_ref[...] = mixed_ref[...]
+    log_out_ref[...] = log_ref[...]
+
+
 def shards(tokens, w_query, w_key, w_value, w_output, query_gain, key_gain):
     vmem = pltpu.VMEM
     bf16, f32 = jnp.bfloat16, jnp.float32
     dma = pltpu.SemaphoreType.DMA
     hbm = pl.BlockSpec(memory_space=pl.ANY)
     local = pl.BlockSpec(memory_space=vmem)
-    return pl.pallas_call(
+    mixed_out, log_sums = pl.pallas_call(
         kernel,
         out_shape=(
             jax.ShapeDtypeStruct((OUT_ROWS, D), bf16),
@@ -479,6 +484,16 @@
         tokens, w_query, w_key.T, w_value.T, w_output,
         query_gain.reshape(1, HEAD), key_gain.reshape(1, HEAD),
     )
+    return pl.pallas_call(
+        hand_over,
+        out_shape=(
+            jax.ShapeDtypeStruct(mixed_out.shape, mixed_out.dtype),
+            jax.ShapeDtypeStruct(log_sums.shape, log_sums.dtype),
+        ),
+        in_specs=[local, local],
+        out_specs=(local, local),
+        name="hand_over",
+    )(mixed_out, log_sums)
 
 
 def solution(mesh):

time: 57.4 us -> 56.5 us (0.984)
  local copies, waits for them, and re-layouts: 2.21 us -> 0 us
  Pallas kernels: 54.4 us -> 55.6 us
    unnamed x4 -> x0, local copies, waits for them, and re-layouts: 2.21 us -> none
    pallas_call x0 -> x1, Pallas kernels: none -> 1.62 us  [shards(): pl.pallas_call(hand_over, out_shape=(jax.ShapeDtypeStruct(mixed_out.shape...]
where the time goes in v3:
time: 56.5 us; the launch traced here: 56.3 us
  Pallas kernels  55.6 us (98%)
  between operations  0.64 us (1%)
    pallas_call x1, Pallas kernels, shards(): pl.pallas_call(kernel, out_shape=(jax.ShapeDtypeStruct((OUT_ROWS, D), bf1...  54 us
    pallas_call x1, Pallas kernels, shards(): pl.pallas_call(hand_over, out_shape=(jax.ShapeDtypeStruct(mixed_out.shape...  1.62 us

profile of v3, /device:TPU:1, one launch (start us, length us, event | category | flops | bytes accessed | tf_op | source)
XLA Modules:
  0.0 56.3 jit_solution(11947461062076242970)
XLA Ops:
  0.6 54.0 %layer.1 = (bf16[48,2048]{1,0:T(8,128)(2,1)}, f32[4,192]{1,0:T(4,128)}) custom-call(bf16[192,2048]{1,0:T(8,128)(2,1)} %tok_hbm.1, bf16[2048,256]{1,0:T(8,128)(2,1)} %wq_hbm.1, bf16[64,2048]{1,0:T(8,128)(2,1)} %bitcast.4, bf16[64,2048]{1,0:T(8,128)(2,1)} %bitcast.5, bf16[256,2048]{1,0:T(8,128)(2,1)} %wo_hbm.1, f32[1,64]{1,0:T(1,128)} %bitcast.6, f32[1,64]{1,0:T(1,128)} %bitcast.7), custom_call_target="tpu_custom_call" | custom-call | tf_op jit(solution)/shard_map/layer/pallas_call | solution.py:436
  54.7 1.6 %hand_over.1 = (bf16[48,2048]{1,0:T(8,128)(2,1)}, f32[4,192]{1,0:T(4,128)}) custom-call(bf16[48,2048]{1,0:T(8,128)(2,1)} %get-tuple-element.4.mixed_ref, f32[4,192]{1,0:T(4,128)} %get-tuple-element.5.log_ref), custom_call_target="tpu_custom_call" | custom-call | tf_op jit(solution)/shard_map/hand_over/pallas_call | solution.py:487
